TPU v7x, 512 devices: a whole 4x8x8 slice. The times are simulated.
512 devices in a mesh: sp: 64 (over z, y), tp: 8 (over x, core).
Axes of the slice: x: 4, y: 8, z: 8, core: 2. Of those that a mesh axis runs over, the one named last changes fastest.
Arguments:
- features: bfloat16 [16384, 2048], P('sp'), may hold values from -16 to 16
- value_weight: bfloat16 [2048, 1024], P(None, 'tp'), may hold values from -0.125 to 0.125
- queries: bfloat16 [16384, 512], P('sp', 'tp'), may hold values from -9 to 9
- key_vectors: bfloat16 [16384, 512], P('sp', 'tp'), may hold values from -0.17 to 0.17
- log_input: float32 [2, 8, 16384], P(None, 'tp', 'sp'), may hold values from -6 to 100
- log_forget: float32 [2, 8, 16384], P(None, 'tp', 'sp'), may hold values from -3 to 0, as said below
- out_grad: bfloat16 [16384, 1024], P('sp', 'tp'), may hold values from -6 to 6
Outputs:
- grad_queries: bfloat16 [16384, 512], P('sp', 'tp')
- grad_keys: bfloat16 [16384, 512], P('sp', 'tp')
- grad_log_input: float32 [2, 8, 16384], P(None, 'tp', 'sp')
- grad_log_forget: float32 [2, 8, 16384], P(None, 'tp', 'sp')
- grad_weight: float32 [2048, 1024], P('sp', 'tp')
- grad_features: bfloat16 [16384, 2048], P(('sp', 'tp'))
Inputs may be any that keep to these rules, and one draw needn't show every extreme that they name: `log_forget`: every entry is below zero.
All inputs are finite; a program needn't handle non-finite values.
Results may differ from a plain program's by a relative error of at most 0.013.
Values may be sent and summed in bfloat16 or wider, within the bound.
A program may use at most 64 MiB of HBM per device.

v0:
```python
import math

import jax
import jax.numpy as jnp
from jax import lax
from jax.sharding import PartitionSpec as P

DK = 64
DV = 128


peak_exponent = lax.Precision.HIGHEST
very_low = -1e30


def sent_to_all(value, axis):
    copies = jnp.broadcast_to(value, (lax.axis_size(axis), *value.shape))
    return lax.all_to_all(copies, axis, split_axis=0, concat_axis=0, tiled=True)


def joined_along(parts, dim):
    lengths = list(parts.shape[1:])
    lengths[dim] *= parts.shape[0]
    return jnp.moveaxis(parts, 0, dim).reshape(lengths)


def gathered_copies(value, axis, dim):
    parts = sent_to_all(value, axis)
    return joined_along(parts, dim)


def side_by_side(arrays, axis, dim, along):
    widths = [math.prod(a.shape[along:]) for a in arrays]
    both = jnp.concatenate(
        [a.reshape(*a.shape[:along], w) for a, w in zip(arrays, widths)], axis=along
    )
    result = lax.all_gather(both, axis, axis=dim, tiled=True)
    parts = jnp.split(result, [sum(widths[:k]) for k in range(1, len(widths))], axis=along)
    return tuple(
        (b.reshape(*result.shape[:along], *a.shape[along:]) for a, b in zip(arrays, parts))
    )


def split_up(value, dim, size):
    before, after = (value.shape[:dim], value.shape[dim + 1 :])
    return jnp.moveaxis(value.reshape(*before, size, -1, *after), dim, 0)


def summed_on_arrival(value, axis, dim):
    size = lax.axis_size(axis)
    parts = lax.all_to_all(split_up(value, dim, size), axis, 0, 0, tiled=True)
    return jnp.sum(parts.astype(jnp.float32), axis=0)


def summarize(float_keys, float_values, log_in, log_fg):
    cumulative = jnp.cumsum(log_fg, axis=1)
    decay_sum = cumulative[:, -1]
    exponent = decay_sum[:, None] - cumulative + log_in
    top_log = jnp.max(exponent, axis=1)
    weight = jnp.exp(exponent - top_log[:, None])
    weighted_terms = float_keys * weight[:, :, None]
    memory_matrix = jnp.einsum(
        "cxr,cxy->cry", weighted_terms, float_values, precision=peak_exponent
    )
    normalizer = jnp.sum(weighted_terms, axis=1)
    return (cumulative, (decay_sum, memory_matrix, normalizer, top_log))


def empty_state(head_count, rows_count, width):
    return (
        jnp.zeros((head_count,), jnp.float32),
        jnp.zeros((head_count, rows_count, width), jnp.float32),
        jnp.zeros((head_count, rows_count), jnp.float32),
        jnp.full((head_count,), very_low, jnp.float32),
    )


def forward_part(query_b, keys_b, values_b, grad_b, log_in, cumulative, incoming):
    incoming_memory, normalizer_in, top_in = incoming
    float_query = query_b.astype(jnp.float32)
    float_keys = keys_b.astype(jnp.float32)
    float_values = values_b.astype(jnp.float32)
    grad_f = grad_b.astype(jnp.float32)
    length = cumulative.shape[1]
    places = lax.iota(jnp.int32, length)
    causal_mask = (places[:, None] >= places[None, :])[None]
    exponent = jnp.where(
        causal_mask, cumulative[:, :, None] - cumulative[:, None, :] + log_in[:, None, :], very_low
    )
    carry_log = cumulative + top_in[:, None]
    top_log = jnp.maximum(carry_log, jnp.max(exponent, axis=2))
    weight = jnp.where(causal_mask, jnp.exp(exponent - top_log[:, :, None]), 0.0)
    carried_over = jnp.exp(carry_log - top_log)
    scores = jnp.einsum("htk,hsk->hts", query_b, keys_b, preferred_element_type=jnp.float32)
    scored = weight * scores
    numerator_term = carried_over[..., None] * jnp.einsum(
        "gsd,gdi->gsi", float_query, incoming_memory, precision=peak_exponent
    ) + jnp.einsum("hts,hsv->htv", scored, float_values, precision=peak_exponent)
    denominator = carried_over * jnp.sum(float_query * normalizer_in[:, None, :], axis=2) + jnp.sum(
        scored, axis=2
    )
    floor_value = jnp.exp(-top_log)
    divisor = jnp.maximum(jnp.abs(denominator), floor_value)
    hidden = numerator_term / divisor[..., None]
    numerator_gradient = grad_f / divisor[..., None]
    grad_denom = jnp.where(
        jnp.abs(denominator) > floor_value,
        -jnp.sign(denominator) * jnp.sum(grad_f * hidden, axis=2) / divisor,
        0.0,
    )
    raw_pairing = jnp.einsum("htv,hsv->hts", grad_b, values_b, preferred_element_type=jnp.float32)
    pairing = raw_pairing / divisor[..., None] + grad_denom[..., None]
    masked = weight * pairing
    grad_query = jnp.einsum(
        "hts,hsk->htk", masked, float_keys, precision=peak_exponent
    ) + carried_over[..., None] * (
        jnp.einsum("pfr,pdr->pdf", incoming_memory, numerator_gradient, precision=peak_exponent)
        + normalizer_in[:, None, :] * grad_denom[..., None]
    )
    key_local = jnp.einsum("hts,htk->hsk", masked, float_query, precision=peak_exponent)
    value_local = jnp.einsum("hts,htv->hsv", scored, numerator_gradient, precision=peak_exponent)
    row_total = jnp.sum(numerator_gradient * numerator_term, axis=2) + grad_denom * denominator
    back_log = cumulative - top_log
    back_top = jnp.max(back_log, axis=1)
    reverse_weight_factor = jnp.exp(back_log - back_top[:, None])
    memory_gradient = jnp.einsum(
        "cxr,cxy->cry",
        float_query * reverse_weight_factor[..., None],
        numerator_gradient,
        precision=peak_exponent,
    )
    normalizer_gradient = jnp.sum(
        float_query * (reverse_weight_factor * grad_denom)[..., None], axis=1
    )
    return (
        grad_query,
        key_local,
        value_local,
        row_total,
        (memory_gradient, normalizer_gradient, back_top),
    )


def backward_part(
    float_keys,
    float_values,
    log_in,
    cumulative,
    decay_sum,
    key_local,
    value_local,
    row_total,
    incoming_state,
    incoming_grad,
):
    incoming_memory, normalizer_in, top_in = incoming_state
    memory_gradient, normalizer_gradient, grad_top = incoming_grad
    scaling = jnp.exp(log_in + decay_sum[:, None] - cumulative + grad_top[:, None])
    passed_key_sum = (
        jnp.einsum("xqy,xty->xtq", memory_gradient, float_values, precision=peak_exponent)
        + normalizer_gradient[:, None, :]
    )
    passed_value_sum = jnp.einsum(
        "nfp,nxf->nxp", memory_gradient, float_keys, precision=peak_exponent
    )
    grad_key = key_local + scaling[..., None] * passed_key_sum
    grad_value = value_local + scaling[..., None] * passed_value_sum
    local_column = jnp.sum(float_keys * key_local, axis=2)
    carried_column = scaling * jnp.sum(float_keys * passed_key_sum, axis=2)
    grad_in = local_column + carried_column
    across = jnp.exp(top_in + decay_sum + grad_top) * (
        jnp.sum(incoming_memory * memory_gradient, axis=(1, 2))
        + jnp.sum(normalizer_in * normalizer_gradient, axis=1)
    )
    suffix = jnp.flip(jnp.cumsum(jnp.flip(row_total - local_column, 1), axis=1), 1)
    prefix = jnp.cumsum(carried_column, axis=1) - carried_column
    grad_fg = suffix + prefix + across[:, None]
    return (grad_key, grad_value, grad_in, grad_fg)


def make_folder(totals, device_place, takes_lower, running, portion):
    before = jnp.cumsum(totals, axis=0) - totals
    mine_before = lax.dynamic_index_in_dim(before, device_place, 0, keepdims=False)
    mine_total = lax.dynamic_index_in_dim(totals, device_place, 0, keepdims=False)
    lower_flag = jnp.array(takes_lower)[None, :, None]
    memory_run, normal_run, top_run = running
    memory_piece, normal_piece, top_piece = portion
    width = top_piece.shape[0]
    row_places = lax.iota(jnp.int32, width)
    log_lower = mine_before[None] - before - totals
    log_upper = before - mine_before[None] - mine_total[None]
    include = jnp.where(
        lower_flag,
        (row_places < device_place)[:, None, None],
        (row_places > device_place)[:, None, None],
    )
    log_gap = jnp.where(lower_flag, log_lower, log_upper)
    candidate = jnp.where(include, log_gap + top_piece, very_low)
    top_new = jnp.maximum(top_run, jnp.max(candidate, axis=0))
    keep_old = jnp.exp(top_run - top_new)
    factor = jnp.where(include, jnp.exp(candidate - top_new[None]), 0.0)
    memory_new = keep_old[..., None, None] * memory_run + jnp.sum(
        factor[..., None, None] * memory_piece, axis=0
    )
    normal_new = keep_old[..., None] * normal_run + jnp.sum(
        factor[..., None] * normal_piece, axis=0
    )
    return (memory_new, normal_new, top_new)


def to_heads(tensor, head_count):
    tokens = tensor.shape[0]
    return tensor.reshape(tokens, head_count, -1).transpose(1, 0, 2)


def body(features, value_weight, queries, key_vectors, log_input, log_forget, out_grad):
    head_count = value_weight.shape[1] // DV
    tokens = features.shape[0]
    values = jnp.dot(features, value_weight, preferred_element_type=jnp.float32).astype(
        jnp.bfloat16
    )
    query_h = to_heads(queries, head_count)
    key_h = to_heads(key_vectors, head_count)
    value_h = to_heads(values, head_count)
    grad_h = to_heads(out_grad, head_count)
    oriented = []
    for direction in range(2):
        packed = [query_h, key_h, value_h, grad_h, log_input[direction], log_forget[direction]]
        if direction == 1:
            packed = [jnp.flip(tensor, 1) for tensor in packed]
        oriented.append(packed)
    cumul_list = []
    summary_list = []
    keys_list = []
    values_list = []
    for direction in range(2):
        packed = oriented[direction]
        float_keys = packed[1].astype(jnp.float32)
        float_values = packed[2].astype(jnp.float32)
        keys_list.append(float_keys)
        values_list.append(float_values)
        cumulative, summary = summarize(float_keys, float_values, packed[4], packed[5])
        cumul_list.append(cumulative)
        summary_list.append(summary)
    start_state = empty_state(head_count, DK, DV)
    device_place = lax.axis_index("sp")
    totals = gathered_copies(jnp.stack([summary_list[0][0], summary_list[1][0]])[None], "sp", 0)
    stacked = tuple(
        (
            jnp.stack([summary_list[0][member], summary_list[1][member]])[None]
            for member in (1, 2, 3)
        )
    )
    state_start = tuple((jnp.stack([tensor, tensor]) for tensor in start_state[1:]))
    folded = make_folder(
        totals,
        device_place,
        (True, False),
        state_start,
        side_by_side((stacked[0], stacked[1], stacked[2]), "sp", 0, 3),
    )
    states = [tuple((tensor[0] for tensor in folded)), tuple((tensor[1] for tensor in folded))]
    forward_results = []
    for direction in range(2):
        packed = oriented[direction]
        forward_results.append(
            forward_part(
                packed[0],
                packed[1],
                packed[2],
                packed[3],
                packed[4],
                cumul_list[direction],
                states[direction],
            )
        )
    grad_stacked = tuple(
        (
            jnp.stack([forward_results[0][4][member], forward_results[1][4][member]])[None]
            for member in (0, 1, 2)
        )
    )
    grad_folded = make_folder(
        totals,
        device_place,
        (False, True),
        state_start,
        side_by_side((grad_stacked[0], grad_stacked[1], grad_stacked[2]), "sp", 0, 3),
    )
    grads_in = [
        tuple((tensor[0] for tensor in grad_folded)),
        tuple((tensor[1] for tensor in grad_folded)),
    ]
    outputs = []
    for direction in range(2):
        packed = oriented[direction]
        grad_query, key_local, value_local, row_total, unused = forward_results[direction]
        grad_key, grad_value, grad_in, grad_fg = backward_part(
            keys_list[direction],
            values_list[direction],
            packed[4],
            cumul_list[direction],
            summary_list[direction][0],
            key_local,
            value_local,
            row_total,
            states[direction],
            grads_in[direction],
        )
        result = (grad_query, grad_key, grad_value, grad_in, grad_fg)
        if direction == 1:
            result = tuple((jnp.flip(tensor, 1) for tensor in result))
        outputs.append(result)
    grad_q = outputs[0][0] + outputs[1][0]
    grad_k = outputs[0][1] + outputs[1][1]
    grad_v = outputs[0][2] + outputs[1][2]
    grad_queries = grad_q.transpose(1, 0, 2).reshape(tokens, head_count * DK).astype(jnp.bfloat16)
    grad_keys = grad_k.transpose(1, 0, 2).reshape(tokens, head_count * DK).astype(jnp.bfloat16)
    grad_values = grad_v.transpose(1, 0, 2).reshape(tokens, head_count * DV).astype(jnp.bfloat16)
    grad_log_input = jnp.stack([outputs[0][3], outputs[1][3]])
    grad_log_forget = jnp.stack([outputs[0][4], outputs[1][4]])
    grad_weight = summed_on_arrival(
        lax.dot_general(
            features, grad_values, (((0,), (0,)), ((), ())), preferred_element_type=jnp.float32
        ).astype(jnp.bfloat16),
        "sp",
        0,
    )
    grad_features = lax.psum_scatter(
        lax.dot_general(
            grad_values, value_weight, (((1,), (1,)), ((), ())), preferred_element_type=jnp.float32
        ).astype(jnp.bfloat16),
        "tp",
        scatter_dimension=0,
        tiled=True,
    )
    return (grad_queries, grad_keys, grad_log_input, grad_log_forget, grad_weight, grad_features)


def solution(mesh):
    placed = (
        P("sp", None),
        P(None, "tp"),
        P("sp", "tp"),
        P("sp", "tp"),
        P(None, "tp", "sp"),
        P(None, "tp", "sp"),
        P("sp", "tp"),
    )
    return jax.shard_map(
        body,
        mesh=mesh,
        in_specs=placed,
        out_specs=(
            P("sp", "tp"),
            P("sp", "tp"),
            P(None, "tp", "sp"),
            P(None, "tp", "sp"),
            P("sp", "tp"),
            P(("sp", "tp"), None),
        ),
        check_vma=False,
    )
```

profile of v0, /device:TPU:6, one launch (start us, length us, event | category | flops | bytes accessed | tf_op | source)
XLA Modules:
  0.0 291.5 jit_solution(12225190388918076369)
XLA Ops:
  7.2 0.8 fusion.87
  8.0 0.7 fusion.86
  8.7 1.5 convolution_convert_fusion.2
  10.3 0.9 reverse.24
  12.5 1.9 fusion.77
  14.4 1.4 subtract_exponential_fusion.5
  15.8 0.9 fusion.22
  16.7 0.9 fusion.21
  19.3 1.2 fusion.82
  20.6 1.3 subtract_exponential_fusion.4
  22.2 1.4 maximum_bitcast_fusion
  23.7 0.8 concatenate.8
  24.5 1.4 maximum_reduce_fusion
  26.6 16.6 %all-to-all-start = ((f32[64,1,2,1]{2,3,1,0:T(1,128)}), f32[64,1,2,1]{2,3,1,0:T(1,128)S(1)}, u32[]{:S(2)}, u32[]{:S(2)}) async-start(f32[64,1,2,1]{2,3,1,0:T(1,128)} %broadcast_in_dim.180), calls=%async_computation | async-start | bytes 65536 | tf_op jit(solution)/shard_map/all_to_all | solution.py:18
  43.7 0.9 reverse.27
  44.6 0.9 copy.162
  45.7 9.4 %all-to-all-done = f32[64,1,2,1]{2,3,1,0:T(1,128)S(1)} async-done(((f32[64,1,2,1]{2,3,1,0:T(1,128)}), f32[64,1,2,1]{2,3,1,0:T(1,128)S(1)}, u32[]{:S(2)}, u32[]{:S(2)}) %all-to-all-start) | async-done | bytes 544 | tf_op jit(solution)/shard_map/all_to_all | solution.py:18
  55.6 60.4 %all-gather.3.cloned.1.call-done = f32[64,2,1,8257]{3,1,2,0:T(2,128)} async-done(((f32[1,2,1,8257]{3,1,2,0:T(2,128)}), f32[64,2,1,8257]{3,1,2,0:T(2,128)}) %all-gather.3.cloned.1.call-update) | async-done | bytes 4227600 | tf_op jit(solution)/shard_map/all_gather | solution.py:37
  116.1 1.0 split.24
  117.3 1.0 fusion.35
  118.9 1.3 fusion.74
  120.8 0.7 fusion.61
  121.6 0.7 select_select_fusion.6
  122.3 1.3 fusion.76
  124.4 1.0 fusion.38
  125.9 4.1 %fusion.1 = f32[2,8192]{1,0:T(2,128)S(1)} fusion(f32[64,2,1,8257]{3,1,2,0:T(2,128)} %all-gather.3.cloned.1.call-done, f32[64,2]{1,0:T(8,128)S(1)} %copy.165), kind=kLoop, calls=%fused_computation.3 | loop fusion | flops 2080768 | bytes 4260352 | tf_op jit(solution)/shard_map/reduce_sum | solution.py:202
  130.0 2.6 copy.186
  132.6 2.8 copy.167
  140.5 1.4 maximum_bitcast_fusion.1
  142.1 0.8 concatenate.9
  147.6 0.9 fusion.18
  148.4 78.1 %all-gather.5.cloned.1.call-done = f32[64,2,1,8257]{3,1,2,0:T(2,128)} async-done(((f32[1,2,1,8257]{3,1,2,0:T(2,128)}), f32[64,2,1,8257]{3,1,2,0:T(2,128)}) %all-gather.5.cloned.1.call-update) | async-done | bytes 4227600 | tf_op jit(solution)/shard_map/all_gather | solution.py:37
  226.5 1.0 split.27
  228.9 1.0 fusion.37
  230.7 4.1 %fusion = f32[2,8192]{1,0:T(2,128)S(1)} fusion(f32[64,2,1,8257]{3,1,2,0:T(2,128)} %all-gather.5.cloned.1.call-done, f32[64,2]{1,0:T(8,128)S(1)} %copy.174), kind=kLoop, calls=%fused_computation.1 | loop fusion | flops 2080768 | bytes 4260352 | tf_op jit(solution)/shard_map/reduce_sum | solution.py:202
  234.8 2.6 copy.187
  237.4 2.9 copy.176
  240.7 1.9 fusion.83
  243.1 1.2 add_exponential_fusion.1
  246.4 0.8 fusion.26
  248.8 1.2 multiply_add_fusion.1
  251.8 1.4 convolution_convert_fusion
  253.6 1.0 copy.182
  254.6 8.7 %all-to-all-start.1 = ((bf16[64,32,128]{2,1,0:T(8,128)(2,1)}), bf16[64,32,128]{2,1,0:T(8,128)(2,1)S(1)}, u32[]{:S(2)}, u32[]{:S(2)}) async-start(bf16[64,32,128]{2,1,0:T(8,128)(2,1)} %bitcast.124), calls=%async_computation.1 | async-start | bytes 1048576 | tf_op jit(solution)/shard_map/all_to_all | solution.py:51
  269.5 1.2 add_bitcast_fusion.1
  271.3 8.0 %all-to-all-done.1 = bf16[64,32,128]{2,1,0:T(8,128)(2,1)S(1)} async-done(((bf16[64,32,128]{2,1,0:T(8,128)(2,1)}), bf16[64,32,128]{2,1,0:T(8,128)(2,1)S(1)}, u32[]{:S(2)}, u32[]{:S(2)}) %all-to-all-start.1) | async-done | bytes 524320 | tf_op jit(solution)/shard_map/all_to_all | solution.py:51
  279.3 0.7 convert_reduce_fusion
  280.0 5.0 %reduce-scatter.2.cloned.1.call-done = bf16[32,2048]{1,0:T(8,128)(2,1)} async-done(((bf16[256,2048]{1,0:T(8,128)(2,1)}), bf16[32,2048]{1,0:T(8,128)(2,1)}) %reduce-scatter.2.cloned.1.call-update) | async-done | bytes 131088 | tf_op jit(solution)/shard_map/reduce_scatter | solution.py:329
  (149 shorter events, 27.2 us)
Async XLA Ops:
  7.2 1.5 copy-start
  7.2 108.9 %all-gather.3.cloned.1.call-start = ((), (), s32[]{:S(2)}) async-start(), calls=%async_computation.3 | async-start | bytes 4326400 | tf_op jit(solution)/shard_map/all_gather | solution.py:37
  26.6 28.5 %all-to-all-start = ((f32[64,1,2,1]{2,3,1,0:T(1,128)}), f32[64,1,2,1]{2,3,1,0:T(1,128)S(1)}, u32[]{:S(2)}, u32[]{:S(2)}) async-start(f32[64,1,2,1]{2,3,1,0:T(1,128)} %broadcast_in_dim.180), calls=%async_computation | async-start | bytes 65536 | tf_op jit(solution)/shard_map/all_to_all | solution.py:18
  43.1 183.4 %all-gather.5.cloned.1.call-start = ((), (), s32[]{:S(2)}) async-start(), calls=%async_computation.4 | async-start | bytes 4326400 | tf_op jit(solution)/shard_map/all_gather | solution.py:37
  130.0 5.6 %copy-start.2 = (bf16[256,64]{0,1:T(8,128)(2,1)S(1)}, bf16[256,64]{0,1:T(8,128)(2,1)}, u32[]{:S(2)}) copy-start(bf16[256,64]{0,1:T(8,128)(2,1)} %param.12) | copy-start | bytes 98308
  130.0 5.6 %copy-start.3 = (bf16[256,64]{0,1:T(8,128)(2,1)S(1)}, bf16[256,64]{0,1:T(8,128)(2,1)}, u32[]{:S(2)}) copy-start(bf16[256,64]{0,1:T(8,128)(2,1)} %param.11) | copy-start | bytes 98308
  135.6 11.5 %copy-start.4 = (bf16[256,128]{1,0:T(8,128)(2,1)S(1)}, bf16[256,128]{1,0:T(8,128)(2,1)}, u32[]{:S(2)}) copy-start(bf16[256,128]{1,0:T(8,128)(2,1)} %param.15) | copy-start | bytes 196612
  139.0 88.7 %copy-start.6 = (pred[2]{0:T(512)(128)(4,1)S(1)}, pred[2]{0:T(512)(128)(4,1)}, u32[]{:S(2)}) copy-start(pred[2]{0:T(512)(128)(4,1)} %constant.45.clone) | copy-start | bytes 10
  142.9 142.2 %reduce-scatter.2.cloned.1.call-start = ((), (), s32[]{:S(2)}) async-start(), calls=%async_computation.5 | async-start | bytes 1179648 | tf_op jit(solution)/shard_map/reduce_scatter | solution.py:329
  234.8 14.0 %copy-start.5 = (f32[2,1,256]{2,1,0:T(1,128)S(1)}, f32[2,1,256]{2,1,0:T(1,128)}, u32[]{:S(2)}) copy-start(f32[2,1,256]{2,1,0:T(1,128)} %param.13) | copy-start | bytes 6148
  237.4 14.4 %copy-start.1 = (bf16[2048,128]{1,0:T(8,128)(2,1)S(1)}, bf16[2048,128]{1,0:T(8,128)(2,1)}, u32[]{:S(2)}) copy-start(bf16[2048,128]{1,0:T(8,128)(2,1)} %param.10) | copy-start | bytes 1572868
  254.6 24.7 %all-to-all-start.1 = ((bf16[64,32,128]{2,1,0:T(8,128)(2,1)}), bf16[64,32,128]{2,1,0:T(8,128)(2,1)S(1)}, u32[]{:S(2)}, u32[]{:S(2)}) async-start(bf16[64,32,128]{2,1,0:T(8,128)(2,1)} %bitcast.124), calls=%async_computation.1 | async-start | bytes 1048576 | tf_op jit(solution)/shard_map/all_to_all | solution.py:51
Sparse Core Ops, SparseCore 0:
  24.6 91.4 all-gather.2
  143.0 83.4 all-gather.4
  253.4 31.5 reduce-scatter.1
where the time goes:
time: 296 us; the launch traced here: 292 us
  waiting for transfers between devices  161 us (54%)
  other arithmetic  45 us (15%)
  local copies, waits for them, and re-layouts  27.9 us (9%)
  starting transfers between devices  25.6 us (9%)
  between operations  20.7 us (7%)
  matrix products  11.4 us (4%)
    all_gather x2, waiting for transfers between devices, side_by_side(): result = lax.all_gather(both, axis, axis=dim, tiled=True)  139 us
    all_to_all x1, starting transfers between devices, sent_to_all(): return lax.all_to_all(copies, axis, split_axis=0, concat_axis=0, tiled=True)  16.6 us
    all_to_all x1, waiting for transfers between devices, sent_to_all(): return lax.all_to_all(copies, axis, split_axis=0, concat_axis=0, tiled=True)  9.36 us
    all_to_all x1, starting transfers between devices, summed_on_arrival(): parts = lax.all_to_all(split_up(value, dim, size), axis, 0, 0, tiled=True)  8.67 us
    reduce_sum x2, other arithmetic, make_folder(): jnp.sum(factor[..., None, None] * memory_piece, axis=0)  8.19 us
    all_to_all x1, waiting for transfers between devices, summed_on_arrival(): parts = lax.all_to_all(split_up(value, dim, size), axis, 0, 0, tiled=True)  8.04 us
    unnamed x19, local copies, waits for them, and re-layouts  6.4 us
  transfers between devices with their start and end apart: 5, of which 5 were waited for; matrix products, arithmetic and copies ran while one was open for 5% of the time, Pallas kernels for 0%

commit v1 on v0

v1 whole, which is shorter than its diff:
```python
import jax
import jax.numpy as jnp
from jax import lax
from jax.experimental import pallas as pl
from jax.experimental.pallas import tpu as pltpu
from jax.sharding import PartitionSpec as P

DK = 64
DV = 128
TOK = 256
D = 2048
SIDE = 8
N_TP = 8
ROWS = D // 64

LOW = -1e30
F32 = jnp.float32
BF16 = jnp.bfloat16
MESH = pl.DeviceIdType.MESH

(N1, N2, M1, M2, M3, G1, G2, G3, H1, H2, A1, B1, A2, B2, VX, VC, GV, KINDS) = range(18)


def dot(a, b, da, db):
    return lax.dot_general(a, b, (((da,), (db,)), ((), ())), preferred_element_type=F32)


def halves(x):
    high = x.astype(BF16)
    return high, (x - high.astype(F32)).astype(BF16)


def dot_left(x, b, da, db):
    high, low = halves(x)
    return dot(high, b, da, db) + dot(low, b, da, db)


def dot_right(a, x, da, db):
    high, low = halves(x)
    return dot(a, high, da, db) + dot(a, low, da, db)


def kernel(
    f_ref, vw_ref, q_ref, k_ref, li_ref, lf_ref, g_ref,
    gq_out, gk_out, gi_out, gf_out, gw_out, gx_out,
    v_s, ft, w_s, s_s, r_s, p_s, u_s,
    n_send, n_buf, nz_send, nz_buf,
    m_send, m_buf, mz_send, mz_buf, mr_send, mr_buf,
    g_send, g_buf, gz_send, gz_buf, gr_send, gr_buf,
    h_send, h_buf, hz_send, hz_buf,
    wa_send, wa_buf, wb_send, wb_buf, wa2_send, wa2_buf, wb2_send, wb2_buf,
    vall, gv_s, gv_buf, ssem, rsem, lsem,
):
    sp = lax.axis_index("sp")
    tp = lax.axis_index("tp")
    z, y = lax.div(sp, SIDE), lax.rem(sp, SIDE)
    x, core = lax.div(tp, 2), lax.rem(tp, 2)

    def peer_id(axis, p):
        if axis == "y":
            return {"sp": z * SIDE + p}
        if axis == "z":
            return {"sp": p * SIDE + y}
        return {"tp": p}

    own = {"y": y, "z": z, "tp": tp}

    def copy(kind, axis, p, src, dst, slot):
        return pltpu.make_async_remote_copy(
            src_ref=src, dst_ref=dst, send_sem=ssem.at[kind, p], recv_sem=rsem.at[kind, slot],
            device_id=peer_id(axis, p), device_id_type=MESH,
        )

    def send_all(kind, axis, src_of, buf):
        me = own[axis]

        def step(i, c):
            p = lax.rem(me + i, SIDE)
            copy(kind, axis, p, src_of(p), buf.at[me], me).start()
            return c

        lax.fori_loop(1, SIDE, step, 0)

    def recv_all(kind, axis, buf):
        me = own[axis]

        def step(i, c):
            p = lax.rem(me + i, SIDE)
            copy(kind, axis, p, buf.at[p], buf.at[p], p).wait_recv()
            return c

        lax.fori_loop(1, SIDE, step, 0)

    def sent_all(kind, axis, src_of, buf):
        me = own[axis]

        def step(i, c):
            p = lax.rem(me + i, SIDE)
            copy(kind, axis, p, src_of(p), buf.at[me], me).wait_send()
            return c

        lax.fori_loop(1, SIDE, step, 0)

    barrier = pltpu.get_barrier_semaphore()
    for axis in ("y", "z", "tp"):
        def greet(i, c, axis=axis):
            p = lax.rem(own[axis] + i, SIDE)
            pl.semaphore_signal(barrier, inc=1, device_id=peer_id(axis, p), device_id_type=MESH)
            return c

        lax.fori_loop(1, SIDE, greet, 0)

    place = pltpu.make_async_copy(vw_ref, vall.at[tp], lsem)
    place.start()

    values = jnp.dot(f_ref[...], vw_ref[...], preferred_element_type=F32).astype(BF16)
    v_s[...] = values
    at_t = lax.broadcasted_iota(jnp.int32, (TOK, TOK), 0)
    at_s = lax.broadcasted_iota(jnp.int32, (TOK, TOK), 1)
    same = at_t == at_s
    reach = (at_s <= at_t, at_s >= at_t)
    lane = lax.broadcasted_iota(jnp.int32, (1, 2 * DK), 1)
    first = lane < DK
    sub = lax.broadcasted_iota(jnp.int32, (8, 2 * DK), 0)

    def column(row):
        return jnp.sum(jnp.where(same, row, 0.0), axis=1, keepdims=True)

    def row_of(col):
        return jnp.sum(jnp.where(same, col, 0.0), axis=0, keepdims=True)

    def pack(a, b):
        return jnp.where(first, a, b)

    def half_sum(packed):
        return (
            jnp.sum(jnp.where(first, packed, 0.0), axis=1, keepdims=True),
            jnp.sum(jnp.where(first, 0.0, packed), axis=1, keepdims=True),
        )

    c_col, i_row, c_row, end, ending, decay, top = [], [], [], [], [], [], []
    for d in range(2):
        l_row = lf_ref[d]
        in_row = li_ref[d]
        c = jnp.sum(jnp.where(reach[d], l_row, 0.0), axis=1, keepdims=True)
        cr = row_of(c)
        total = c[TOK - 1 :, :] if d == 0 else c[:1, :]
        e = total - c + column(in_row)
        peak = jnp.max(e, axis=0, keepdims=True)
        c_col.append(c)
        c_row.append(cr)
        i_row.append(in_row)
        ending.append(e)
        decay.append(total)
        top.append(peak)
    key2 = jnp.concatenate([k_ref[...], k_ref[...]], axis=1).astype(F32)
    weighted = key2 * pack(jnp.exp(ending[0] - top[0]), jnp.exp(ending[1] - top[1]))
    norm = jnp.sum(weighted, axis=0, keepdims=True)
    decay2 = pack(decay[0], decay[1])
    top2 = pack(top[0], top[1])

    def tile(a, b, c):
        return jnp.where(sub == 0, a, jnp.where(sub == 1, b, jnp.where(sub == 2, c, 0.0)))

    n_send[...] = tile(norm, decay2, top2)
    n_buf[y] = n_send[...]
    pl.semaphore_wait(barrier, 3 * (SIDE - 1))
    send_all(N1, "y", lambda p: n_send, n_buf)

    memory = dot_left(weighted, values, 0, 0)
    m_send[:, 0] = memory[:DK].reshape(SIDE, 8, DV)
    m_send[:, 1] = memory[DK:].reshape(SIDE, 8, DV)
    m_buf[y] = m_send[y]
    send_all(M1, "y", lambda p: m_send.at[p], m_buf)

    mate = x * 2 + (1 - core)
    for i in range(1, 4):
        p = lax.rem(x + i, 4) * 2 + core
        copy(VX, "tp", p, vw_ref, vall.at[tp], tp).start()
    copy(VC, "tp", mate, vw_ref, vall.at[tp], tp).start()

    scores = dot(q_ref[...], k_ref[...], 1, 1)
    s_s[...] = scores
    r_s[...] = dot(g_ref[...], v_s[...], 1, 1)
    m_local, den_local, num_local = [], [], []
    for d in range(2):
        e = jnp.where(reach[d], c_col[d] - c_row[d] + i_row[d], LOW)
        peak = jnp.max(e, axis=1, keepdims=True)
        w = jnp.exp(e - peak)
        w_s[d] = w
        ws = w * s_s[...]
        m_local.append(peak)
        den_local.append(jnp.sum(ws, axis=1, keepdims=True))
        num_local.append(jnp.sum(ws * r_s[...], axis=1, keepdims=True))

    def element(tiles, i, flip, rows):
        near, far = tiles[i], tiles[SIDE - 1 - i]
        take = first if not flip else jnp.logical_not(first)
        return [jnp.where(take, near[r : r + 1], far[r : r + 1]) for r in rows]

    def included(i, at, flip):
        low = jnp.where(i < at, 1, 0)
        high = jnp.where(SIDE - 1 - i > at, 1, 0)
        if flip:
            low, high = high, low
        return jnp.where(first, low, high) > 0

    empty = jnp.full((1, 2 * DK), LOW, F32)

    def chain(decays, tops, start, masks):
        run, past, factors = start, jnp.zeros((1, 2 * DK), F32), []
        for i in range(SIDE):
            dec, high = decays[i], tops[i]
            if masks is not None:
                dec = jnp.where(masks[i], dec, 0.0)
                high = jnp.where(masks[i], high, LOW)
            new = jnp.maximum(run + dec, high)
            keep = jnp.exp(run + dec - new)
            add = jnp.exp(high - new)
            if masks is not None:
                add = jnp.where(masks[i], add, 0.0)
            factors.append((keep, add))
            run, past = new, past + dec
        return run, past, factors

    def fold_rows(rows, factors):
        acc = jnp.zeros((1, 2 * DK), F32)
        for row, (keep, add) in zip(rows, factors):
            acc = keep * acc + add * row
        return acc

    def both(factor):
        return factor[:, :1], factor[:, DK : DK + 1]

    def fold_tiles(buf, factors, flip, start, store):
        acc = list(start)
        for i in range(SIDE):
            keep, add = both(factors[i][0]), both(factors[i][1])
            places = (i, SIDE - 1 - i) if not flip else (SIDE - 1 - i, i)
            for d in range(2):
                if store is not None:
                    store[places[d], d] = acc[d]
                acc[d] = keep[d] * acc[d] + add[d] * buf[places[d], d]
        return acc

    zero_tile = jnp.zeros((8, DV), F32)

    recv_all(N1, "y", n_buf)
    tiles_y = [n_buf[i] for i in range(SIDE)]
    els = [element(tiles_y, i, False, (0, 1, 2)) for i in range(SIDE)]
    norms_y, decays_y, tops_y = zip(*els)
    row_top, row_decay, total_f = chain(decays_y, tops_y, empty, None)
    row_norm = fold_rows(norms_y, total_f)
    nz_send[...] = tile(row_norm, row_decay, row_top)
    nz_buf[z] = nz_send[...]
    send_all(N2, "z", lambda p: nz_send, nz_buf)
    pre_top, pre_decay, pre_f = chain(
        decays_y, tops_y, empty, [included(i, y, False) for i in range(SIDE)]
    )
    pre_norm = fold_rows(norms_y, pre_f)

    recv_all(M1, "y", m_buf)
    sums = fold_tiles(m_buf, total_f, False, (zero_tile, zero_tile), None)
    mz_send[0] = sums[0]
    mz_send[1] = sums[1]
    mz_buf[z] = mz_send[...]
    send_all(M2, "z", lambda p: mz_send, mz_buf)

    recv_all(N2, "z", nz_buf)
    tiles_z = [nz_buf[i] for i in range(SIDE)]
    els = [element(tiles_z, i, False, (0, 1, 2)) for i in range(SIDE)]
    norms_z, decays_z, tops_z = zip(*els)
    far_top, unused, far_f = chain(
        decays_z, tops_z, empty, [included(i, z, False) for i in range(SIDE)]
    )
    far_norm = fold_rows(norms_z, far_f)
    in_top = jnp.maximum(far_top + pre_decay, pre_top)
    in_norm = jnp.exp(far_top + pre_decay - in_top) * far_norm + jnp.exp(pre_top - in_top) * pre_norm

    query2 = jnp.concatenate([q_ref[...], q_ref[...]], axis=1).astype(F32)
    qn = half_sum(query2 * in_norm)
    in_tops = both(in_top)
    alpha, beta, inv, den, big, back, back_top = [], [], [], [], [], [], []
    for d in range(2):
        carry = c_col[d] + in_tops[d]
        m = jnp.maximum(carry, m_local[d])
        a = jnp.exp(m_local[d] - m)
        b = jnp.exp(carry - m)
        dn = b * qn[d] + a * den_local[d]
        floor = jnp.exp(-m)
        size = jnp.abs(dn)
        blog = c_col[d] - m
        peak = jnp.max(blog, axis=0, keepdims=True)
        alpha.append(a)
        beta.append(b)
        den.append(dn)
        big.append(size > floor)
        inv.append(1.0 / jnp.maximum(size, floor))
        back_top.append(peak)
        back.append(jnp.exp(blog - peak))
    back2 = pack(back_top[0], back_top[1])
    slope = dot_left(query2 * pack(back[0] * inv[0], back[1] * inv[1]), g_ref[...], 0, 0)
    g_send[:, 0] = slope[:DK].reshape(SIDE, 8, DV)
    g_send[:, 1] = slope[DK:].reshape(SIDE, 8, DV)
    g_send[:, 2] = jnp.broadcast_to(tile(back2, back2, back2), (SIDE, 8, DV))
    g_buf[y] = g_send[y]
    send_all(G1, "y", lambda p: g_send.at[p], g_buf)

    unused, unused, into_f = chain(decays_y, tops_y, far_top, None)
    recv_all(M2, "z", mz_buf)
    far = fold_tiles(mz_buf, far_f, False, (zero_tile, zero_tile), None)
    fold_tiles(m_buf, into_f, False, far, mr_send)
    mr_buf[y] = mr_send[y]
    send_all(M3, "y", lambda p: mr_send.at[p], mr_buf)

    u_s[...] = (w_s[0] * (alpha[0] * inv[0]) + w_s[1] * (alpha[1] * inv[1])) * s_s[...]
    v_local = dot_left(u_s[...], g_ref[...], 0, 0)

    recv_all(G1, "y", g_buf)
    els = [
        jnp.where(first, g_buf[SIDE - 1 - i, 2, 0:1], g_buf[i, 2, 0:1]) for i in range(SIDE)
    ]
    back_decays_y = decays_y[::-1]
    g_top, unused, g_total_f = chain(back_decays_y, els, empty, None)
    back_y = els
    sums = fold_tiles(g_buf, g_total_f, True, (zero_tile, zero_tile), None)
    gz_send[0] = sums[0]
    gz_send[1] = sums[1]
    gz_send[2] = tile(g_top, g_top, g_top)
    gz_buf[z] = gz_send[...]
    send_all(G2, "z", lambda p: gz_send, gz_buf)
    g_pre_top, g_pre_decay, g_pre_f = chain(
        back_decays_y, back_y, empty, [included(i, y, True) for i in range(SIDE)]
    )

    recv_all(M3, "y", mr_buf)
    in_mem = jnp.concatenate(
        [mr_buf[:, 0].reshape(DK, DV), mr_buf[:, 1].reshape(DK, DV)], axis=0
    )
    cross = dot_right(g_ref[...], in_mem, 1, 1)
    gq = half_sum(query2 * cross)
    gd, row_total = [], []
    for d in range(2):
        along = (beta[d] * gq[d] + alpha[d] * num_local[d]) * inv[d]
        signed = jnp.where(den[d] > 0.0, -along, along) * inv[d]
        gd.append(jnp.where(big[d], signed, 0.0))
        row_total.append(jnp.where(big[d], 0.0, along))
    n_grad = jnp.sum(query2 * pack(back[0] * gd[0], back[1] * gd[1]), axis=0, keepdims=True)
    h_send[...] = jnp.broadcast_to(n_grad, (8, DV))
    h_buf[y] = h_send[...]
    send_all(H1, "y", lambda p: h_send, h_buf)

    recv_all(G2, "z", gz_buf)
    back_decays_z = decays_z[::-1]
    back_z = [
        jnp.where(first, gz_buf[SIDE - 1 - i, 2, 0:1], gz_buf[i, 2, 0:1]) for i in range(SIDE)
    ]
    g_far_top, unused, g_far_f = chain(
        back_decays_z, back_z, empty, [included(i, z, True) for i in range(SIDE)]
    )
    far = fold_tiles(gz_buf, g_far_f, True, (zero_tile, zero_tile), None)
    unused, unused, g_into_f = chain(back_decays_y, back_y, g_far_top, None)
    fold_tiles(g_buf, g_into_f, True, far, gr_send)
    gr_buf[y] = gr_send[y]
    send_all(G3, "y", lambda p: gr_send.at[p], gr_buf)

    recv_all(H1, "y", h_buf)
    n_rows_y = [jnp.where(first, h_buf[SIDE - 1 - i, 0:1], h_buf[i, 0:1]) for i in range(SIDE)]
    hz_send[...] = jnp.broadcast_to(fold_rows(n_rows_y, g_total_f), (8, DV))
    hz_buf[z] = hz_send[...]
    send_all(H2, "z", lambda p: hz_send, hz_buf)
    g_pre_norm = fold_rows(n_rows_y, g_pre_f)

    column_sum = []
    for d in range(2):
        part = w_s[d] * (r_s[...] * (alpha[d] * inv[d]) + alpha[d] * gd[d])
        if d == 0:
            p_s[...] = part
        else:
            p_s[...] += part
        column_sum.append(jnp.sum(part * s_s[...], axis=0, keepdims=True))
    p_high, p_low = halves(p_s[...])
    gq_local = dot(p_high, k_ref[...], 1, 0) + dot(p_low, k_ref[...], 1, 0)
    k_local = dot(p_high, q_ref[...], 0, 0) + dot(p_low, q_ref[...], 0, 0)
    carried = cross * pack(beta[0] * inv[0], beta[1] * inv[1]) + in_norm * pack(
        beta[0] * gd[0], beta[1] * gd[1]
    )
    gq_out[...] = (gq_local + carried[:, :DK] + carried[:, DK:]).astype(BF16)

    for j in range(SIDE):
        ft[j] = f_ref[:, j * TOK : (j + 1) * TOK].T

    for i in range(1, 4):
        p = lax.rem(x + i, 4) * 2 + core
        copy(VX, "tp", p, vw_ref, vall.at[p], p).wait_recv()
        pltpu.make_async_remote_copy(
            src_ref=vall.at[p], dst_ref=vall.at[p], send_sem=ssem.at[VC, p],
            recv_sem=rsem.at[VC, p], device_id=peer_id("tp", mate), device_id_type=MESH,
        ).start()

    g_in_top = jnp.maximum(g_far_top + g_pre_decay, g_pre_top)
    g_tops = both(g_in_top)
    scale2 = pack(jnp.exp(ending[0] + g_tops[0]), jnp.exp(ending[1] + g_tops[1]))
    scaled = key2 * scale2
    recv_all(G3, "y", gr_buf)
    in_slope = jnp.concatenate(
        [gr_buf[:, 0].reshape(DK, DV), gr_buf[:, 1].reshape(DK, DV)], axis=0
    )
    slope_high, slope_low = halves(in_slope)
    scaled_high, scaled_low = halves(scaled)
    grad_values = (
        v_local
        + dot(scaled_high, slope_high, 1, 0)
        + dot(scaled_high, slope_low, 1, 0)
        + dot(scaled_low, slope_high, 1, 0)
    ).astype(BF16)
    gv_s[...] = grad_values.reshape(N_TP, TOK // N_TP, DV)
    gv_buf[tp] = gv_s[tp]
    send_all(GV, "tp", lambda p: gv_s.at[p], gv_buf)

    gv_all = gv_s[...].reshape(TOK, DV)
    for i in range(1, SIDE + 1):
        p = lax.rem(z + i, SIDE)
        piece = dot(ft[p], gv_all, 1, 0).astype(BF16).reshape(SIDE, 2, ROWS // 2, DV)
        wa_send[p] = piece[:, 0]
        wb_send[:, p] = piece[:, 1]
        if i < SIDE:
            copy(A1, "z", p, wa_send.at[p], wa_buf.at[z], z).start()
    wa_buf[z] = wa_send[z]
    wb_buf[y] = wb_send[y]
    send_all(B1, "y", lambda p: wb_send.at[p], wb_buf)

    recv_all(H2, "z", hz_buf)
    n_rows_z = [jnp.where(first, hz_buf[SIDE - 1 - i, 0:1], hz_buf[i, 0:1]) for i in range(SIDE)]
    g_far_norm = fold_rows(n_rows_z, g_far_f)
    g_in_norm = (
        jnp.exp(g_far_top + g_pre_decay - g_in_top) * g_far_norm
        + jnp.exp(g_pre_top - g_in_top) * g_pre_norm
    )
    values = v_s[...]
    passed = dot(values, slope_high, 1, 1) + dot(values, slope_low, 1, 1) + g_in_norm
    moved = scale2 * passed
    gk_out[...] = (k_local + moved[:, :DK] + moved[:, DK:]).astype(BF16)
    carried_column = half_sum(scaled * passed)
    pair = in_mem * in_slope
    pair_norm = half_sum(in_norm * g_in_norm)
    for d in range(2):
        gi_out[d] = column_sum[d] + row_of(carried_column[d])
        inner = jnp.sum(
            jnp.sum(pair[d * DK : (d + 1) * DK], axis=0, keepdims=True), axis=1, keepdims=True
        )
        across = jnp.exp(in_tops[d] + decay[d] + g_tops[d]) * (inner + pair_norm[d])
        ahead = row_total[d] - column(column_sum[d])
        span = jnp.where(reach[d], ahead, carried_column[d])
        gf_out[d] = jnp.sum(span, axis=0, keepdims=True) + across

    place.wait()
    for j in range(4):
        p = j * 2 + (1 - core)
        copy(VC, "tp", p, vw_ref, vall.at[p], p).wait_recv()
    recv_all(GV, "tp", gv_buf)
    for j in range(4):
        cols = slice(j * 512, (j + 1) * 512)
        acc = dot(gv_buf[0], vall[0, cols], 1, 1)
        for h in range(1, N_TP):
            acc += dot(gv_buf[h], vall[h, cols], 1, 1)
        gx_out[:, cols] = acc.astype(BF16)

    recv_all(A1, "z", wa_buf)
    wa2_send[...] = jnp.sum(wa_buf[...].astype(F32), axis=0).astype(BF16)
    wa2_buf[y] = wa2_send[y]
    send_all(A2, "y", lambda p: wa2_send.at[p], wa2_buf)
    recv_all(B1, "y", wb_buf)
    wb2_send[...] = jnp.sum(wb_buf[...].astype(F32), axis=0).astype(BF16)
    wb2_buf[z] = wb2_send[z]
    send_all(B2, "z", lambda p: wb2_send.at[p], wb2_buf)
    recv_all(A2, "y", wa2_buf)
    gw_out[: ROWS // 2] = jnp.sum(wa2_buf[...].astype(F32), axis=0)
    recv_all(B2, "z", wb2_buf)
    gw_out[ROWS // 2 :] = jnp.sum(wb2_buf[...].astype(F32), axis=0)

    for kind, axis, src_of, buf in (
        (N1, "y", lambda p: n_send, n_buf),
        (N2, "z", lambda p: nz_send, nz_buf),
        (M1, "y", lambda p: m_send.at[p], m_buf),
        (M2, "z", lambda p: mz_send, mz_buf),
        (M3, "y", lambda p: mr_send.at[p], mr_buf),
        (G1, "y", lambda p: g_send.at[p], g_buf),
        (G2, "z", lambda p: gz_send, gz_buf),
        (G3, "y", lambda p: gr_send.at[p], gr_buf),
        (H1, "y", lambda p: h_send, h_buf),
        (H2, "z", lambda p: hz_send, hz_buf),
        (A1, "z", lambda p: wa_send.at[p], wa_buf),
        (B1, "y", lambda p: wb_send.at[p], wb_buf),
        (A2, "y", lambda p: wa2_send.at[p], wa2_buf),
        (B2, "z", lambda p: wb2_send.at[p], wb2_buf),
        (GV, "tp", lambda p: gv_s.at[p], gv_buf),
    ):
        sent_all(kind, axis, src_of, buf)
    for i in range(1, 4):
        p = lax.rem(x + i, 4) * 2 + core
        copy(VX, "tp", p, vw_ref, vall.at[tp], tp).wait_send()
        copy(VC, "tp", p, vall.at[p], vall.at[p], p).wait_send()
    copy(VC, "tp", mate, vw_ref, vall.at[tp], tp).wait_send()


def body(features, value_weight, queries, key_vectors, log_input, log_forget, out_grad):
    whole = pl.BlockSpec(memory_space=pltpu.VMEM)
    tile = (8, DV)
    part = (ROWS // 2, DV)
    scratch = [
        pltpu.VMEM((TOK, DV), BF16),
        pltpu.VMEM((SIDE, TOK, TOK), BF16),
        pltpu.VMEM((2, TOK, TOK), F32),
        pltpu.VMEM((TOK, TOK), F32),
        pltpu.VMEM((TOK, TOK), F32),
        pltpu.VMEM((TOK, TOK), F32),
        pltpu.VMEM((TOK, TOK), F32),
        pltpu.VMEM(tile, F32),
        pltpu.VMEM((SIDE, *tile), F32),
        pltpu.VMEM(tile, F32),
        pltpu.VMEM((SIDE, *tile), F32),
        pltpu.VMEM((SIDE, 2, *tile), F32),
        pltpu.VMEM((SIDE, 2, *tile), F32),
        pltpu.VMEM((2, *tile), F32),
        pltpu.VMEM((SIDE, 2, *tile), F32),
        pltpu.VMEM((SIDE, 2, *tile), F32),
        pltpu.VMEM((SIDE, 2, *tile), F32),
        pltpu.VMEM((SIDE, 3, *tile), F32),
        pltpu.VMEM((SIDE, 3, *tile), F32),
        pltpu.VMEM((3, *tile), F32),
        pltpu.VMEM((SIDE, 3, *tile), F32),
        pltpu.VMEM((SIDE, 2, *tile), F32),
        pltpu.VMEM((SIDE, 2, *tile), F32),
        pltpu.VMEM(tile, F32),
        pltpu.VMEM((SIDE, *tile), F32),
        pltpu.VMEM(tile, F32),
        pltpu.VMEM((SIDE, *tile), F32),
        pltpu.VMEM((SIDE, SIDE, *part), BF16),
        pltpu.VMEM((SIDE, SIDE, *part), BF16),
        pltpu.VMEM((SIDE, SIDE, *part), BF16),
        pltpu.VMEM((SIDE, SIDE, *part), BF16),
        pltpu.VMEM((SIDE, *part), BF16),
        pltpu.VMEM((SIDE, *part), BF16),
        pltpu.VMEM((SIDE, *part), BF16),
        pltpu.VMEM((SIDE, *part), BF16),
        pltpu.VMEM((N_TP, D, DV), BF16),
        pltpu.VMEM((N_TP, TOK // N_TP, DV), BF16),
        pltpu.VMEM((N_TP, TOK // N_TP, DV), BF16),
        pltpu.SemaphoreType.DMA((KINDS, SIDE)),
        pltpu.SemaphoreType.DMA((KINDS, SIDE)),
        pltpu.SemaphoreType.DMA,
    ]
    return pl.pallas_call(
        kernel,
        out_shape=(
            jax.ShapeDtypeStruct((TOK, DK), BF16),
            jax.ShapeDtypeStruct((TOK, DK), BF16),
            jax.ShapeDtypeStruct((2, 1, TOK), F32),
            jax.ShapeDtypeStruct((2, 1, TOK), F32),
            jax.ShapeDtypeStruct((ROWS, DV), F32),
            jax.ShapeDtypeStruct((TOK // N_TP, D), BF16),
        ),
        in_specs=[whole] * 7,
        out_specs=[whole] * 6,
        scratch_shapes=scratch,
        compiler_params=pltpu.CompilerParams(
            collective_id=0, has_side_effects=True, vmem_limit_bytes=48 * 1024 * 1024
        ),
    )(features, value_weight, queries, key_vectors, log_input, log_forget, out_grad)


def solution(mesh):
    placed = (
        P("sp", None),
        P(None, "tp"),
        P("sp", "tp"),
        P("sp", "tp"),
        P(None, "tp", "sp"),
        P(None, "tp", "sp"),
        P("sp", "tp"),
    )
    return jax.shard_map(
        body,
        mesh=mesh,
        in_specs=placed,
        out_specs=(
            P("sp", "tp"),
            P("sp", "tp"),
            P(None, "tp", "sp"),
            P(None, "tp", "sp"),
            P("sp", "tp"),
            P(("sp", "tp"), None),
        ),
        check_vma=False,
    )
```

time: 296 us -> 66.6 us (0.22); the launches traced: 292 us -> 66.2 us
  waiting for transfers between devices: 161 us -> 0 us
  Pallas kernels: 0 us -> 57.7 us
  other arithmetic: 45 us -> 0 us
  starting transfers between devices: 25.6 us -> 0 us
  local copies, waits for them, and re-layouts: 27.9 us -> 7.8 us
  between operations: 20.7 us -> 0.69 us
  matrix products: 11.4 us -> 0 us
    all_gather x2 -> x0, waiting for transfers between devices: 139 us -> none  [side_by_side(): result = lax.all_gather(both, axis, axis=dim, tiled=True)]
    pallas_call x0 -> x1, Pallas kernels: none -> 57.7 us  [body(): pl.pallas_call(kernel, out_shape=(jax.ShapeDtypeStruct((TOK, DK), BF16),...]
    all_to_all x2 -> x0, starting transfers between devices: 25.3 us -> none  [the longest x1 16.6 us: sent_to_all(): return lax.all_to_all(copies, axis, split_axis=0, concat_axis=0, tiled=True)]
    all_to_all x2 -> x0, waiting for transfers between devices: 17.4 us -> none  [the longest x1 9.36 us: sent_to_all(): return lax.all_to_all(copies, axis, split_axis=0, concat_axis=0, tiled=True)]
    reduce_sum x13 -> x0, other arithmetic: 13.5 us -> none  [the longest x2 8.19 us: make_folder(): jnp.sum(factor[..., None, None] * memory_piece, axis=0)]
    dot_general x27 -> x0, matrix products: 11.4 us -> none  [the longest x1 1.46 us: body(): jnp.dot(features, value_weight, preferred_element_type=jnp.float32)]
    another operation x29 -> x0, other arithmetic: 9.76 us -> none
    reduce_max x8 -> x0, other arithmetic: 7.47 us -> none  [the longest x2 3.18 us: summarize(): top_log = jnp.max(exponent, axis=1)]
  transfers between devices with their start and end apart: 5 -> 0, of which waited for: 5 -> 0; matrix products, arithmetic and copies ran while one was open for 5% -> 0% of each run, Pallas kernels for 0% -> 0%
where the time goes in v1:
time: 66.6 us; the launch traced here: 66.2 us
  Pallas kernels  57.7 us (87%)
  local copies, waits for them, and re-layouts  7.8 us (12%)
  between operations  0.69 us (1%)
    pallas_call x1, Pallas kernels, body(): pl.pallas_call(kernel, out_shape=(jax.ShapeDtypeStruct((TOK, DK), BF16),...  57.7 us
    unnamed x18, local copies, waits for them, and re-layouts  6.38 us
    pallas_call x2, local copies, waits for them, and re-layouts, body(): pl.pallas_call(kernel, out_shape=(jax.ShapeDtypeStruct((TOK, DK), BF16),...  1.42 us

profile of v1, /device:TPU:6, one launch (start us, length us, event | category | flops | bytes accessed | tf_op | source)
XLA Modules:
  0.0 66.2 jit_solution(2393438178352827581)
XLA Ops:
  0.6 0.0 copy-start.5
  0.6 0.9 %copy.13.q_ref = bf16[256,64]{1,0:T(8,128)(2,1)S(1)} copy(bf16[256,64]{0,1:T(8,128)(2,1)} %param.9) | data formatting | bytes 65536 | tf_op args[2]
  1.5 0.0 copy-done.5
  1.5 0.0 copy-start.2
  1.5 0.0 copy-start.3
  1.6 0.0 copy-start.4
  1.6 0.1 copy.14.k_ref
  1.7 0.7 %copy-done.2 = bf16[256,128]{1,0:T(8,128)(2,1)S(1)} copy-done((bf16[256,128]{1,0:T(8,128)(2,1)S(1)}, bf16[256,128]{1,0:T(8,128)(2,1)}, u32[]{:S(2)}) %copy-start.2) | copy-done | bytes 65560
  2.4 0.0 copy-done.3
  2.4 0.0 copy-done.4
  2.4 0.0 copy-start
  2.4 1.2 %copy-done = bf16[256,2048]{1,0:T(8,128)(2,1)S(1)} copy-done((bf16[256,2048]{1,0:T(8,128)(2,1)S(1)}, bf16[256,2048]{1,0:T(8,128)(2,1)}, u32[]{:S(2)}) %copy-start) | copy-done | bytes 1048600
  3.6 0.0 copy-start.1
  3.6 1.0 %copy-done.1 = bf16[2048,128]{1,0:T(8,128)(2,1)S(1)} copy-done((bf16[2048,128]{1,0:T(8,128)(2,1)S(1)}, bf16[2048,128]{1,0:T(8,128)(2,1)}, u32[]{:S(2)}) %copy-start.1) | copy-done | bytes 524312
  4.6 57.7 %shard_map.118 = (bf16[256,64]{1,0:T(8,128)(2,1)S(1)}, bf16[256,64]{1,0:T(8,128)(2,1)S(1)}, f32[2,1,256]{2,1,0:T(1,128)S(1)}, f32[2,1,256]{2,1,0:T(1,128)S(1)}, ...) custom-call(bf16[256,2048]{1,0:T(8,128)(2,1)S(1)} %copy-done, bf16[2048,128]{1,0:T(8,128)(2,1)S(1)} %copy-done.1, ...), custom_call_target="tpu_custom_call" | custom-call | tf_op jit(solution)/shard_map/pallas_call | solution.py:554
  62.3 0.7 %copy.15 = bf16[256,64]{0,1:T(8,128)(2,1)} copy(bf16[256,64]{1,0:T(8,128)(2,1)S(1)} %get-tuple-element.6) | data formatting | bytes 65536 | tf_op jit(solution)/shard_map/pallas_call | solution.py:554
  63.0 0.7 %copy.16 = bf16[256,64]{0,1:T(8,128)(2,1)} copy(bf16[256,64]{1,0:T(8,128)(2,1)S(1)} %get-tuple-element.7) | data formatting | bytes 65536 | tf_op jit(solution)/shard_map/pallas_call | solution.py:554
  63.7 0.6 copy.21
  64.3 0.6 copy.22
  64.9 0.6 copy.23
  65.5 0.7 copy.24
Async XLA Ops:
  0.6 0.9 %copy-start.5 = (bf16[256,64]{0,1:T(8,128)(2,1)S(1)}, bf16[256,64]{0,1:T(8,128)(2,1)}, u32[]{:S(2)}) copy-start(bf16[256,64]{0,1:T(8,128)(2,1)} %param.10) | copy-start | bytes 98308
  1.5 0.8 %copy-start.2 = (bf16[256,128]{1,0:T(8,128)(2,1)S(1)}, bf16[256,128]{1,0:T(8,128)(2,1)}, u32[]{:S(2)}) copy-start(bf16[256,128]{1,0:T(8,128)(2,1)} %g_ref.1) | copy-start | bytes 196612
  1.5 0.8 %copy-start.3 = (f32[2,1,256]{2,1,0:T(1,128)S(1)}, f32[2,1,256]{2,1,0:T(1,128)}, u32[]{:S(2)}) copy-start(f32[2,1,256]{2,1,0:T(1,128)} %li_ref.1) | copy-start | bytes 6148
  1.6 0.8 %copy-start.4 = (f32[2,1,256]{2,1,0:T(1,128)S(1)}, f32[2,1,256]{2,1,0:T(1,128)}, u32[]{:S(2)}) copy-start(f32[2,1,256]{2,1,0:T(1,128)} %lf_ref.1) | copy-start | bytes 6148
  2.4 1.2 %copy-start = (bf16[256,2048]{1,0:T(8,128)(2,1)S(1)}, bf16[256,2048]{1,0:T(8,128)(2,1)}, u32[]{:S(2)}) copy-start(bf16[256,2048]{1,0:T(8,128)(2,1)} %f_ref.1) | copy-start | bytes 3145732
  3.6 1.0 %copy-start.1 = (bf16[2048,128]{1,0:T(8,128)(2,1)S(1)}, bf16[2048,128]{1,0:T(8,128)(2,1)}, u32[]{:S(2)}) copy-start(bf16[2048,128]{1,0:T(8,128)(2,1)} %vw_ref.1) | copy-start | bytes 1572868

commit v2 on v1

--- a/solution.py
+++ b/solution.py
@@ -18,7 +18,9 @@
 BF16 = jnp.bfloat16
 MESH = pl.DeviceIdType.MESH
 
-(N1, N2, M1, M2, M3, G1, G2, G3, H1, H2, A1, B1, A2, B2, VX, VC, GV, KINDS) = range(18)
+(N1, N2, M1, M2, M3, G1, G2, G3, H1, H2, A1, B1, A2, B2, GV, VL, VR, VA, VB, C0, C1, C2, C3, KINDS) = range(24)
+FAR_FIRST = (4, 3, 5, 2, 6, 1, 7)
+HALF = D // 2
 
 
 def dot(a, b, da, db):
@@ -41,8 +43,9 @@
 
 
 def kernel(
-    f_ref, vw_ref, q_ref, k_ref, li_ref, lf_ref, g_ref,
+    f_in, vw_in, q_in, k_in, li_in, lf_in, g_in,
     gq_out, gk_out, gi_out, gf_out, gw_out, gx_out,
+    f_ref, q_ref, k_ref, li_ref, lf_ref, g_ref,
     v_s, ft, w_s, s_s, r_s, p_s, u_s,
     n_send, n_buf, nz_send, nz_buf,
     m_send, m_buf, mz_send, mz_buf, mr_send, mr_buf,
@@ -56,6 +59,18 @@
     z, y = lax.div(sp, SIDE), lax.rem(sp, SIDE)
     x, core = lax.div(tp, 2), lax.rem(tp, 2)
 
+    loads = [
+        pltpu.make_async_copy(src, dst, lsem.at[n])
+        for n, (src, dst) in enumerate(
+            (
+                (lf_in, lf_ref), (li_in, li_ref), (vw_in, vall.at[tp]), (f_in, f_ref),
+                (k_in, k_ref), (q_in, q_ref), (g_in, g_ref),
+            )
+        )
+    ]
+    for load in loads:
+        load.start()
+
     def peer_id(axis, p):
         if axis == "y":
             return {"sp": z * SIDE + p}
@@ -65,56 +80,36 @@
 
     own = {"y": y, "z": z, "tp": tp}
 
-    def copy(kind, axis, p, src, dst, slot):
+    def copy(kind, axis, p, src, dst):
         return pltpu.make_async_remote_copy(
-            src_ref=src, dst_ref=dst, send_sem=ssem.at[kind, p], recv_sem=rsem.at[kind, slot],
+            src_ref=src, dst_ref=dst, send_sem=ssem.at[kind], recv_sem=rsem.at[kind],
             device_id=peer_id(axis, p), device_id_type=MESH,
         )
 
     def send_all(kind, axis, src_of, buf):
         me = own[axis]
-
-        def step(i, c):
+        for i in FAR_FIRST:
             p = lax.rem(me + i, SIDE)
-            copy(kind, axis, p, src_of(p), buf.at[me], me).start()
-            return c
-
-        lax.fori_loop(1, SIDE, step, 0)
+            copy(kind, axis, p, src_of(p), buf.at[me]).start()
+
+    def all_of(kind, axis, buf):
+        rest = buf.at[pl.ds(0, SIDE - 1)]
+        return copy(kind, axis, lax.rem(own[axis] + 1, SIDE), rest, rest)
 
     def recv_all(kind, axis, buf):
-        me = own[axis]
-
-        def step(i, c):
-            p = lax.rem(me + i, SIDE)
-            copy(kind, axis, p, buf.at[p], buf.at[p], p).wait_recv()
-            return c
-
-        lax.fori_loop(1, SIDE, step, 0)
-
-    def sent_all(kind, axis, src_of, buf):
-        me = own[axis]
-
-        def step(i, c):
-            p = lax.rem(me + i, SIDE)
-            copy(kind, axis, p, src_of(p), buf.at[me], me).wait_send()
-            return c
-
-        lax.fori_loop(1, SIDE, step, 0)
+        all_of(kind, axis, buf).wait_recv()
+
+    def sent_all(kind, axis, buf):
+        all_of(kind, axis, buf).wait_send()
 
     barrier = pltpu.get_barrier_semaphore()
     for axis in ("y", "z", "tp"):
-        def greet(i, c, axis=axis):
+        for i in FAR_FIRST:
             p = lax.rem(own[axis] + i, SIDE)
             pl.semaphore_signal(barrier, inc=1, device_id=peer_id(axis, p), device_id_type=MESH)
-            return c
-
-        lax.fori_loop(1, SIDE, greet, 0)
-
-    place = pltpu.make_async_copy(vw_ref, vall.at[tp], lsem)
-    place.start()
-
-    values = jnp.dot(f_ref[...], vw_ref[...], preferred_element_type=F32).astype(BF16)
-    v_s[...] = values
+
+    loads[0].wait()
+    loads[1].wait()
     at_t = lax.broadcasted_iota(jnp.int32, (TOK, TOK), 0)
     at_s = lax.broadcasted_iota(jnp.int32, (TOK, TOK), 1)
     same = at_t == at_s
@@ -153,7 +148,9 @@
         ending.append(e)
         decay.append(total)
         top.append(peak)
-    key2 = jnp.concatenate([k_ref[...], k_ref[...]], axis=1).astype(F32)
+    loads[4].wait()
+    key2 = jnp.concatenate([k_ref[...], k_ref[...]], axis=0).astype(F32).T
+    key = key2[:, :DK].astype(BF16)
     weighted = key2 * pack(jnp.exp(ending[0] - top[0]), jnp.exp(ending[1] - top[1]))
     norm = jnp.sum(weighted, axis=0, keepdims=True)
     decay2 = pack(decay[0], decay[1])
@@ -164,6 +161,10 @@
 
     n_send[...] = tile(norm, decay2, top2)
     n_buf[y] = n_send[...]
+    loads[2].wait()
+    loads[3].wait()
+    values = jnp.dot(f_ref[...], vall[tp], preferred_element_type=F32).astype(BF16)
+    v_s[...] = values
     pl.semaphore_wait(barrier, 3 * (SIDE - 1))
     send_all(N1, "y", lambda p: n_send, n_buf)
 
@@ -174,13 +175,18 @@
     send_all(M1, "y", lambda p: m_send.at[p], m_buf)
 
     mate = x * 2 + (1 - core)
-    for i in range(1, 4):
-        p = lax.rem(x + i, 4) * 2 + core
-        copy(VX, "tp", p, vw_ref, vall.at[tp], tp).start()
-    copy(VC, "tp", mate, vw_ref, vall.at[tp], tp).start()
-
-    scores = dot(q_ref[...], k_ref[...], 1, 1)
-    s_s[...] = scores
+    left = lax.rem(x + 3, 4) * 2 + core
+    right = lax.rem(x + 1, 4) * 2 + core
+    across_x = lax.rem(x + 2, 4) * 2 + core
+    mine = vall.at[tp]
+    copy(VL, "tp", right, mine, mine).start()
+    copy(VR, "tp", left, mine, mine).start()
+    copy(C0, "tp", mate, mine, mine).start()
+
+    loads[5].wait()
+    loads[6].wait()
+    query2 = jnp.concatenate([q_ref[...], q_ref[...]], axis=0).astype(F32).T
+    s_s[...] = dot(q_ref[...], k_ref[...], 0, 0)
     r_s[...] = dot(g_ref[...], v_s[...], 1, 1)
     m_local, den_local, num_local = [], [], []
     for d in range(2):
@@ -277,7 +283,6 @@
     in_top = jnp.maximum(far_top + pre_decay, pre_top)
     in_norm = jnp.exp(far_top + pre_decay - in_top) * far_norm + jnp.exp(pre_top - in_top) * pre_norm
 
-    query2 = jnp.concatenate([q_ref[...], q_ref[...]], axis=1).astype(F32)
     qn = half_sum(query2 * in_norm)
     in_tops = both(in_top)
     alpha, beta, inv, den, big, back, back_top = [], [], [], [], [], [], []
@@ -316,6 +321,16 @@
     u_s[...] = (w_s[0] * (alpha[0] * inv[0]) + w_s[1] * (alpha[1] * inv[1])) * s_s[...]
     v_local = dot_left(u_s[...], g_ref[...], 0, 0)
 
+    from_left, from_right = vall.at[left], vall.at[right]
+    copy(VL, "tp", left, mine, from_left).wait_recv()
+    part = vall.at[left, pl.ds(0, HALF)]
+    copy(VA, "tp", right, part, part).start()
+    copy(C1, "tp", mate, from_left, from_left).start()
+    copy(VR, "tp", right, mine, from_right).wait_recv()
+    part = vall.at[right, pl.ds(HALF, HALF)]
+    copy(VB, "tp", left, part, part).start()
+    copy(C2, "tp", mate, from_right, from_right).start()
+
     recv_all(G1, "y", g_buf)
     els = [
         jnp.where(first, g_buf[SIDE - 1 - i, 2, 0:1], g_buf[i, 2, 0:1]) for i in range(SIDE)
@@ -380,23 +395,21 @@
             p_s[...] += part
         column_sum.append(jnp.sum(part * s_s[...], axis=0, keepdims=True))
     p_high, p_low = halves(p_s[...])
-    gq_local = dot(p_high, k_ref[...], 1, 0) + dot(p_low, k_ref[...], 1, 0)
-    k_local = dot(p_high, q_ref[...], 0, 0) + dot(p_low, q_ref[...], 0, 0)
+    gq_local = dot(k_ref[...], p_high, 1, 1) + dot(k_ref[...], p_low, 1, 1)
+    k_local = dot(q_ref[...], p_high, 1, 0) + dot(q_ref[...], p_low, 1, 0)
     carried = cross * pack(beta[0] * inv[0], beta[1] * inv[1]) + in_norm * pack(
         beta[0] * gd[0], beta[1] * gd[1]
     )
-    gq_out[...] = (gq_local + carried[:, :DK] + carried[:, DK:]).astype(BF16)
+    turned = carried.T
+    gq_out[...] = (gq_local + turned[:DK] + turned[DK:]).astype(BF16)
 
     for j in range(SIDE):
         ft[j] = f_ref[:, j * TOK : (j + 1) * TOK].T
 
-    for i in range(1, 4):
-        p = lax.rem(x + i, 4) * 2 + core
-        copy(VX, "tp", p, vw_ref, vall.at[p], p).wait_recv()
-        pltpu.make_async_remote_copy(
-            src_ref=vall.at[p], dst_ref=vall.at[p], send_sem=ssem.at[VC, p],
-            recv_sem=rsem.at[VC, p], device_id=peer_id("tp", mate), device_id_type=MESH,
-        ).start()
+    opposite = vall.at[across_x]
+    copy(VA, "tp", left, vall.at[tp, pl.ds(0, HALF)], vall.at[across_x, pl.ds(0, HALF)]).wait_recv()
+    copy(VB, "tp", left, vall.at[tp, pl.ds(0, HALF)], vall.at[across_x, pl.ds(HALF, HALF)]).wait_recv()
+    copy(C3, "tp", mate, opposite, opposite).start()
 
     g_in_top = jnp.maximum(g_far_top + g_pre_decay, g_pre_top)
     g_tops = both(g_in_top)
@@ -425,7 +438,7 @@
         wa_send[p] = piece[:, 0]
         wb_send[:, p] = piece[:, 1]
         if i < SIDE:
-            copy(A1, "z", p, wa_send.at[p], wa_buf.at[z], z).start()
+            copy(A1, "z", p, wa_send.at[p], wa_buf.at[z]).start()
     wa_buf[z] = wa_send[z]
     wb_buf[y] = wb_send[y]
     send_all(B1, "y", lambda p: wb_send.at[p], wb_buf)
@@ -440,7 +453,8 @@
     values = v_s[...]
     passed = dot(values, slope_high, 1, 1) + dot(values, slope_low, 1, 1) + g_in_norm
     moved = scale2 * passed
-    gk_out[...] = (k_local + moved[:, :DK] + moved[:, DK:]).astype(BF16)
+    turned = moved.T
+    gk_out[...] = (k_local + turned[:DK] + turned[DK:]).astype(BF16)
     carried_column = half_sum(scaled * passed)
     pair = in_mem * in_slope
     pair_norm = half_sum(in_norm * g_in_norm)
@@ -454,10 +468,8 @@
         span = jnp.where(reach[d], ahead, carried_column[d])
         gf_out[d] = jnp.sum(span, axis=0, keepdims=True) + across
 
-    place.wait()
-    for j in range(4):
-        p = j * 2 + (1 - core)
-        copy(VC, "tp", p, vw_ref, vall.at[p], p).wait_recv()
+    for kind in (C0, C1, C2, C3):
+        copy(kind, "tp", mate, mine, vall.at[mate]).wait_recv()
     recv_all(GV, "tp", gv_buf)
     for j in range(4):
         cols = slice(j * 512, (j + 1) * 512)
@@ -479,36 +491,41 @@
     recv_all(B2, "z", wb2_buf)
     gw_out[ROWS // 2 :] = jnp.sum(wb2_buf[...].astype(F32), axis=0)
 
-    for kind, axis, src_of, buf in (
-        (N1, "y", lambda p: n_send, n_buf),
-        (N2, "z", lambda p: nz_send, nz_buf),
-        (M1, "y", lambda p: m_send.at[p], m_buf),
-        (M2, "z", lambda p: mz_send, mz_buf),
-        (M3, "y", lambda p: mr_send.at[p], mr_buf),
-        (G1, "y", lambda p: g_send.at[p], g_buf),
-        (G2, "z", lambda p: gz_send, gz_buf),
-        (G3, "y", lambda p: gr_send.at[p], gr_buf),
-        (H1, "y", lambda p: h_send, h_buf),
-        (H2, "z", lambda p: hz_send, hz_buf),
-        (A1, "z", lambda p: wa_send.at[p], wa_buf),
-        (B1, "y", lambda p: wb_send.at[p], wb_buf),
-        (A2, "y", lambda p: wa2_send.at[p], wa2_buf),
-        (B2, "z", lambda p: wb2_send.at[p], wb2_buf),
-        (GV, "tp", lambda p: gv_s.at[p], gv_buf),
+    for kind, axis, buf in (
+        (N1, "y", n_buf), (N2, "z", nz_buf), (M1, "y", m_buf), (M2, "z", mz_buf), (M3, "y", mr_buf),
+        (G1, "y", g_buf), (G2, "z", gz_buf), (G3, "y", gr_buf), (H1, "y", h_buf), (H2, "z", hz_buf),
+        (A1, "z", wa_buf), (B1, "y", wb_buf), (A2, "y", wa2_buf), (B2, "z", wb2_buf),
+        (GV, "tp", gv_buf),
     ):
-        sent_all(kind, axis, src_of, buf)
-    for i in range(1, 4):
-        p = lax.rem(x + i, 4) * 2 + core
-        copy(VX, "tp", p, vw_ref, vall.at[tp], tp).wait_send()
-        copy(VC, "tp", p, vall.at[p], vall.at[p], p).wait_send()
-    copy(VC, "tp", mate, vw_ref, vall.at[tp], tp).wait_send()
+        sent_all(kind, axis, buf)
+    for kind in (VL, VR, C0, C1, C2, C3):
+        copy(kind, "tp", mate, mine, mine).wait_send()
+    for kind in (VA, VB):
+        part = vall.at[tp, pl.ds(0, HALF)]
+        copy(kind, "tp", mate, part, part).wait_send()
+
+
+def writer(*refs):
+    srcs, dsts, sems = refs[:6], refs[6:12], refs[12]
+    copies = [pltpu.make_async_copy(a, b, sems.at[n]) for n, (a, b) in enumerate(zip(srcs, dsts))]
+    for c in copies:
+        c.start()
+    for c in copies:
+        c.wait()
 
 
 def body(features, value_weight, queries, key_vectors, log_input, log_forget, out_grad):
     whole = pl.BlockSpec(memory_space=pltpu.VMEM)
+    outside = pl.BlockSpec(memory_space=pltpu.HBM)
     tile = (8, DV)
     part = (ROWS // 2, DV)
     scratch = [
+        pltpu.VMEM((TOK, D), BF16),
+        pltpu.VMEM((DK, TOK), BF16),
+        pltpu.VMEM((DK, TOK), BF16),
+        pltpu.VMEM((2, 1, TOK), F32),
+        pltpu.VMEM((2, 1, TOK), F32),
+        pltpu.VMEM((TOK, DV), BF16),
         pltpu.VMEM((TOK, DV), BF16),
         pltpu.VMEM((SIDE, TOK, TOK), BF16),
         pltpu.VMEM((2, TOK, TOK), F32),
@@ -547,27 +564,37 @@
         pltpu.VMEM((N_TP, D, DV), BF16),
         pltpu.VMEM((N_TP, TOK // N_TP, DV), BF16),
         pltpu.VMEM((N_TP, TOK // N_TP, DV), BF16),
-        pltpu.SemaphoreType.DMA((KINDS, SIDE)),
-        pltpu.SemaphoreType.DMA((KINDS, SIDE)),
-        pltpu.SemaphoreType.DMA,
+        pltpu.SemaphoreType.DMA((KINDS,)),
+        pltpu.SemaphoreType.DMA((KINDS,)),
+        pltpu.SemaphoreType.DMA((7,)),
     ]
-    return pl.pallas_call(
+    shapes = (
+        jax.ShapeDtypeStruct((DK, TOK), BF16),
+        jax.ShapeDtypeStruct((DK, TOK), BF16),
+        jax.ShapeDtypeStruct((2, 1, TOK), F32),
+        jax.ShapeDtypeStruct((2, 1, TOK), F32),
+        jax.ShapeDtypeStruct((ROWS, DV), F32),
+        jax.ShapeDtypeStruct((TOK // N_TP, D), BF16),
+    )
+    results = pl.pallas_call(
         kernel,
-        out_shape=(
-            jax.ShapeDtypeStruct((TOK, DK), BF16),
-            jax.ShapeDtypeStruct((TOK, DK), BF16),
-            jax.ShapeDtypeStruct((2, 1, TOK), F32),
-            jax.ShapeDtypeStruct((2, 1, TOK), F32),
-            jax.ShapeDtypeStruct((ROWS, DV), F32),
-            jax.ShapeDtypeStruct((TOK // N_TP, D), BF16),
-        ),
-        in_specs=[whole] * 7,
+        out_shape=shapes,
+        in_specs=[outside] * 7,
         out_specs=[whole] * 6,
         scratch_shapes=scratch,
         compiler_params=pltpu.CompilerParams(
-            collective_id=0, has_side_effects=True, vmem_limit_bytes=48 * 1024 * 1024
+            collective_id=0, has_side_effects=True, vmem_limit_bytes=62 * 1024 * 1024
         ),
-    )(features, value_weight, queries, key_vectors, log_input, log_forget, out_grad)
+    )(features, value_weight, queries.T, key_vectors.T, log_input, log_forget, out_grad)
+    written = pl.pallas_call(
+        writer,
+        out_shape=shapes,
+        in_specs=[whole] * 6,
+        out_specs=[outside] * 6,
+        scratch_shapes=[pltpu.SemaphoreType.DMA((6,))],
+        compiler_params=pltpu.CompilerParams(vmem_limit_bytes=4 * 1024 * 1024),
+    )(*results)
+    return (written[0].T, written[1].T, *written[2:])
 
 
 def solution(mesh):

time: 66.6 us -> 57.3 us (0.86)
  Pallas kernels: 57.7 us -> 52.4 us
  local copies, waits for them, and re-layouts: 7.8 us -> 3.81 us
    pallas_call x1 -> x2, Pallas kernels: 57.7 us -> 52.4 us  [the longest x1 51.7 us: body(): pl.pallas_call(kernel, out_shape=shapes, in_specs=[outside] * 7, out_spec...]
    unnamed x18 -> x12, local copies, waits for them, and re-layouts: 6.38 us -> 3.81 us
    pallas_call x2 -> x0, local copies, waits for them, and re-layouts: 1.42 us -> none  [body(): pl.pallas_call(kernel, out_shape=(jax.ShapeDtypeStruct((TOK, DK), BF16),...]
where the time goes in v2:
time: 57.3 us; the launch traced here: 56.9 us
  Pallas kernels  52.4 us (91%)
  local copies, waits for them, and re-layouts  3.81 us (7%)
  between operations  0.66 us (1%)
    pallas_call x1, Pallas kernels, body(): pl.pallas_call(kernel, out_shape=shapes, in_specs=[outside] * 7, out_spec...  51.7 us
    unnamed x12, local copies, waits for them, and re-layouts  3.81 us

profile of v2, /device:TPU:6, one launch (start us, length us, event | category | flops | bytes accessed | tf_op | source)
XLA Modules:
  0.0 56.9 jit_solution(14817547087461577932)
XLA Ops:
  0.6 51.7 %shard_map.118 = (bf16[64,256]{1,0:T(8,128)(2,1)}, bf16[64,256]{1,0:T(8,128)(2,1)}, f32[2,1,256]{2,1,0:T(1,128)}, f32[2,1,256]{2,1,0:T(1,128)}, f32[32,128]{1,0:T(8,128)}, /*index=5*/bf16[32,2048]{1,0:T(8,128)(2,1)}) custom-call(bf16[256,2048]{1,0:T(8,128)(2,1)} %f_in.1, bf16[2048,128]{1,0:T(8,128)(2,1)} %vw_in.1, bf16[64,256]{1,0:T(8,128)(2,1)} %bitcast.4, ...), custom_call_target="tpu_custom_call" | custom-call | tf_op jit(solution)/shard_map/pallas_call | solution.py:579
  52.3 0.0 copy-start.5
  52.3 0.0 copy-start.4
  52.4 0.6 %copy-done.5 = f32[2,1,256]{2,1,0:T(1,128)S(1)} copy-done((f32[2,1,256]{2,1,0:T(1,128)S(1)}, f32[2,1,256]{2,1,0:T(1,128)}, u32[]{:S(2)}) %copy-start.5) | copy-done | bytes 2072
  53.0 0.0 copy-done.4
  53.0 0.0 copy-start
  53.0 0.9 %copy-done = bf16[32,2048]{1,0:T(8,128)(2,1)S(1)} copy-done((bf16[32,2048]{1,0:T(8,128)(2,1)S(1)}, bf16[32,2048]{1,0:T(8,128)(2,1)}, u32[]{:S(2)}) %copy-start) | copy-done | bytes 131096
  53.9 0.0 copy-start.1
  53.9 0.8 %copy-done.1 = bf16[64,256]{1,0:T(8,128)(2,1)S(1)} copy-done((bf16[64,256]{1,0:T(8,128)(2,1)S(1)}, bf16[64,256]{1,0:T(8,128)(2,1)}, u32[]{:S(2)}) %copy-start.1) | copy-done | bytes 32792
  54.7 0.0 copy-start.2
  54.7 0.8 %copy-done.2 = bf16[64,256]{1,0:T(8,128)(2,1)S(1)} copy-done((bf16[64,256]{1,0:T(8,128)(2,1)S(1)}, bf16[64,256]{1,0:T(8,128)(2,1)}, u32[]{:S(2)}) %copy-start.2) | copy-done | bytes 32792
  55.4 0.0 copy-start.3
  55.4 0.7 %copy-done.3 = f32[32,128]{1,0:T(8,128)S(1)} copy-done((f32[32,128]{1,0:T(8,128)S(1)}, f32[32,128]{1,0:T(8,128)}, u32[]{:S(2)}) %copy-start.3) | copy-done | bytes 16408
  56.2 0.7 %shard_map.119 = (bf16[64,256]{1,0:T(8,128)(2,1)}, bf16[64,256]{1,0:T(8,128)(2,1)}, f32[2,1,256]{2,1,0:T(1,128)}, f32[2,1,256]{2,1,0:T(1,128)}, f32[32,128]{1,0:T(8,128)}, /*index=5*/bf16[32,2048]{1,0:T(8,128)(2,1)}) custom-call(bf16[64,256]{1,0:T(8,128)(2,1)S(1)} %copy-done.1, bf16[64,256]{1,0:T(8,128)(2,1)S(1)} %copy-done.2, f32[2,1,256]{2,1,0:T(1,128)S(1)} %copy-done.4, ...), custom_call_target="tpu_custom_call" | custom-call | tf_op jit(solution)/shard_map/pallas_call | solution.py:589
Async XLA Ops:
  52.3 0.7 %copy-start.5 = (f32[2,1,256]{2,1,0:T(1,128)S(1)}, f32[2,1,256]{2,1,0:T(1,128)}, u32[]{:S(2)}) copy-start(f32[2,1,256]{2,1,0:T(1,128)} %get-tuple-element.21.refs_3_) | copy-start | bytes 6148
  52.3 0.7 %copy-start.4 = (f32[2,1,256]{2,1,0:T(1,128)S(1)}, f32[2,1,256]{2,1,0:T(1,128)}, u32[]{:S(2)}) copy-start(f32[2,1,256]{2,1,0:T(1,128)} %get-tuple-element.20.refs_2_) | copy-start | bytes 6148
  53.0 0.9 %copy-start = (bf16[32,2048]{1,0:T(8,128)(2,1)S(1)}, bf16[32,2048]{1,0:T(8,128)(2,1)}, u32[]{:S(2)}) copy-start(bf16[32,2048]{1,0:T(8,128)(2,1)} %get-tuple-element.23.refs_5_) | copy-start | bytes 393220
  53.9 0.8 %copy-start.1 = (bf16[64,256]{1,0:T(8,128)(2,1)S(1)}, bf16[64,256]{1,0:T(8,128)(2,1)}, u32[]{:S(2)}) copy-start(bf16[64,256]{1,0:T(8,128)(2,1)} %get-tuple-element.18.refs_0_) | copy-start | bytes 98308
  54.7 0.8 %copy-start.2 = (bf16[64,256]{1,0:T(8,128)(2,1)S(1)}, bf16[64,256]{1,0:T(8,128)(2,1)}, u32[]{:S(2)}) copy-start(bf16[64,256]{1,0:T(8,128)(2,1)} %get-tuple-element.19.refs_1_) | copy-start | bytes 98308
  55.4 0.7 %copy-start.3 = (f32[32,128]{1,0:T(8,128)S(1)}, f32[32,128]{1,0:T(8,128)}, u32[]{:S(2)}) copy-start(f32[32,128]{1,0:T(8,128)} %get-tuple-element.22.refs_4_) | copy-start | bytes 49156
